TPU v7x, 32 devices: a whole 2x2x4 slice. The times are simulated.
32 devices in a mesh: grp: 2 (over x), ep: 16 (over z, y, core).
Axes of the slice: x: 2, y: 2, z: 4, core: 2. Of those that a mesh axis runs over, the one named last changes fastest.
Arguments:
- tokens: bfloat16 [4096, 2048], P(('grp', 'ep')), parts along dimension 0, may hold values from -6 to 6
- norm_gain: float32 [2048], replicated, may hold values from 0.1 to 1.9
- expert_ids: int32 [4096, 2], P(('grp', 'ep')), parts along dimension 0, may hold values from 0 to 3, as said below
- mix_weights: float32 [4096, 2], P(('grp', 'ep')), parts along dimension 0, may hold values from 0.2 to 1
- gate_weight: bfloat16 [2048, 28672], P(None, 'ep'), may hold values from -0.125 to 0.125
- up_weight: bfloat16 [2048, 28672], P(None, 'ep'), may hold values from -0.125 to 0.125
- down_weight: bfloat16 [28672, 2048], P('ep'), may hold values from -0.0625 to 0.0625
Outputs:
- mixed: bfloat16 [4096, 2048], P(('grp', 'ep')), parts along dimension 0
There are 2 independent parts, one for each index of `grp`. A program takes and returns all parts, laid end to end along the dimension named above; an argument that names none is the same for every part. Nothing has to cross between parts.
Inputs may be any that keep to these rules, and one draw needn't show every extreme that they name: `expert_ids`: each token names 2 different experts. In the rows of one device no expert is named by more than 80 rows, and in every draw each expert is named by exactly 80 rows of some device.
All inputs are finite; a program needn't handle non-finite values.
Results may differ from a plain program's by a relative error of at most 0.008.
Values may be sent and summed in bfloat16 or wider, within the bound.
A program may use at most 128 MiB of HBM per device.

v0:
```python
import functools

import jax
import jax.numpy as jnp
from jax import lax
from jax.experimental import pallas as pl
from jax.experimental.pallas import tpu as pltpu
from jax.sharding import PartitionSpec as P

SPLIT = 4
CHUNK = 16
f32, bf16 = jnp.float32, jnp.bfloat16


def tile_of(extent, most):
    tile = most
    while extent % tile:
        tile //= 2
    return tile


def kernel(
    experts,
    tok_ref, gain_ref, ids_ref, mix_ref, wg_hbm, wu_hbm, wd_hbm,
    out_ref,
    wg, wu, wd, normed, disp, xin, hid, part, r1, r2s, r2r, r3s, home, acc,
    w_sem, zs_sem, zr_sem, ys_sem, yr_sem, cs_sem, cr_sem, ds_sem, dr_sem,
    r1s_sem, r1r_sem, r2s_sem, r2r_sem, r3s_sem, r3r_sem,
):
    me = lax.axis_index("ep")
    z = me // SPLIT
    y = (me // 2) % 2
    c = me % 2
    rows, width = tok_ref.shape
    cap = disp.shape[1]
    nq = cap // CHUNK
    ff = wg.shape[1]
    top = ids_ref.shape[0]
    at_y = {"ep": z * SPLIT + (1 - y) * 2 + c}
    at_c = {"ep": z * SPLIT + y * 2 + (1 - c)}
    mine = c * 2 + y
    other_y = c * 2 + 1 - y
    other_c = (1 - c) * 2 + y
    other_yc = (1 - c) * 2 + 1 - y

    def peer(k):
        shift = jnp.where(k == 0, 0, (k + experts // 2 - 2) % (experts - 1) + 1)
        return z ^ shift

    def at_z(k):
        return {"ep": peer(k) * SPLIT + y * 2 + c}

    def remote(src, dst, send, recv, where):
        return pltpu.make_async_remote_copy(
            src_ref=src, dst_ref=dst, send_sem=send, recv_sem=recv,
            device_id=where, device_id_type=pl.DeviceIdType.MESH,
        )

    def chunk(q):
        return pl.ds(pl.multiple_of(q * CHUNK, CHUNK), CHUNK)

    ft = tile_of(ff, 256)
    nf = ff // ft
    dt = tile_of(width, 256)
    nd = width // dt

    def weight_gu(j):
        cols = pl.ds(pl.multiple_of(j * ft, ft), ft)
        return (
            pltpu.make_async_copy(wg_hbm.at[:, cols], wg.at[:, cols], w_sem.at[0, j]),
            pltpu.make_async_copy(wu_hbm.at[:, cols], wu.at[:, cols], w_sem.at[1, j]),
        )

    weight_d = pltpu.make_async_copy(wd_hbm, wd, w_sem.at[2, 0])

    barrier = pltpu.get_barrier_semaphore()

    for k in range(1, experts):
        pl.semaphore_signal(barrier, inc=1, device_id=at_z(k), device_id_type=pl.DeviceIdType.MESH)
    pl.semaphore_signal(barrier, inc=1, device_id=at_y, device_id_type=pl.DeviceIdType.MESH)
    pl.semaphore_signal(barrier, inc=1, device_id=at_c, device_id_type=pl.DeviceIdType.MESH)

    for j in range(nf):
        for copy in weight_gu(j):
            copy.start()
    weight_d.start()

    step = tile_of(rows, 16)

    @pl.loop(0, rows // step)
    def _(r):
        at = pl.ds(pl.multiple_of(r * step, step), step)
        values = tok_ref[at, :].astype(f32)
        scale = lax.rsqrt(jnp.mean(values * values, axis=-1, keepdims=True) + 1e-06)
        normed[at, :] = (values * scale * gain_ref[...]).astype(bf16)

    lanes = 128
    expert_row = lax.broadcasted_iota(jnp.int32, (lanes, rows), 0)
    named = ids_ref[0:1, :] == expert_row
    weight_t = jnp.where(named, mix_ref[0:1, :], 0.0)
    for k in range(1, top):
        hit = ids_ref[k : k + 1, :] == expert_row
        named = named | hit
        weight_t = weight_t + jnp.where(hit, mix_ref[k : k + 1, :], 0.0)
    named = named.astype(f32)
    first = lax.broadcasted_iota(jnp.int32, (rows, rows), 0)
    second = lax.broadcasted_iota(jnp.int32, (rows, rows), 1)
    upper = (first < second).astype(f32).astype(bf16)
    rank_t = jnp.dot(named.astype(bf16), upper, preferred_element_type=f32)
    rank_t = jnp.where(named > 0.5, rank_t, -1.0)
    rank = jnp.transpose(rank_t)
    weight_c = jnp.transpose(weight_t)
    lane = lax.broadcasted_iota(jnp.int32, (rows, lanes), 1)

    def dispatch(e, dst):
        slot = jnp.sum(jnp.where(expert_row == e, rank_t, 0.0), axis=0, keepdims=True)
        place = lax.broadcasted_iota(jnp.int32, (cap, rows), 0)
        pick = (place == slot.astype(jnp.int32)).astype(f32).astype(bf16)
        wide = tile_of(width, 512)
        for n in range(width // wide):
            cols = slice(n * wide, (n + 1) * wide)
            dst[:, cols] = jnp.dot(pick, normed[:, cols], preferred_element_type=f32).astype(bf16)

    def z_copy(k, q):
        return remote(disp.at[k, chunk(q)], xin.at[z, mine, chunk(q)], zs_sem.at[k, q], zr_sem.at[z, q], at_z(k))

    def z_arrival(k, q):
        p = peer(k)
        return remote(disp.at[k, chunk(q)], xin.at[p, mine, chunk(q)], zs_sem.at[k, q], zr_sem.at[p, q], at_z(k))

    def in_group(sub, send, recv, where):
        def make(k, q):
            slot = xin.at[peer(k), sub, chunk(q)]
            return remote(slot, slot, send.at[k, q], recv.at[k, q], where)

        return make

    y_copy = in_group(mine, ys_sem, yr_sem, at_y)
    y_arrival = in_group(other_y, ys_sem, yr_sem, at_y)
    c_copy = in_group(mine, cs_sem, cr_sem, at_c)
    c_arrival = in_group(other_c, cs_sem, cr_sem, at_c)
    d_copy = in_group(other_y, ds_sem, dr_sem, at_c)
    d_arrival = in_group(other_yc, ds_sem, dr_sem, at_c)

    def r1_copy(k, v, q):
        return remote(
            part.at[k, 1 - c, v, chunk(q)], r1.at[k, v, chunk(q)], r1s_sem.at[k, v, q], r1r_sem.at[k, v, q], at_c
        )

    def r2_copy(k, q):
        return remote(r2s.at[k, chunk(q)], r2r.at[k, chunk(q)], r2s_sem.at[k, q], r2r_sem.at[k, q], at_y)

    def r3_copy(k, q):
        return remote(r3s.at[k, chunk(q)], home.at[z, chunk(q)], r3s_sem.at[k, q], r3r_sem.at[z, q], at_z(k))

    def r3_arrival(k, q):
        p = peer(k)
        return remote(r3s.at[k, chunk(q)], home.at[p, chunk(q)], r3s_sem.at[k, q], r3r_sem.at[p, q], at_z(k))

    def forward_z(k, q):
        @pl.when(k > 0)
        def _():
            z_arrival(k, q).wait_recv()

        y_copy(k, q).start()
        c_copy(k, q).start()

    def forward_y(k, q):
        y_arrival(k, q).wait_recv()
        d_copy(k, q).start()

    def reduce_chip(k, q):
        at = chunk(q)
        r1_copy(k, 1 - y, q).wait_recv()
        r2s[k, at, :] = (part[k, c, 1 - y, at, :].astype(f32) + r1[k, 1 - y, at, :].astype(f32)).astype(bf16)
        r2_copy(k, q).start()

    def reduce_group(k, q):
        @pl.when(q < nq)
        def _():
            at = chunk(q)
            r1_copy(k, y, q).wait_recv()
            r2_copy(k, q).wait_recv()
            total = (
                part[k, c, y, at, :].astype(f32) + r1[k, y, at, :].astype(f32) + r2r[k, at, :].astype(f32)
            ).astype(bf16)

            @pl.when(k == 0)
            def _():
                home[z, at, :] = total

            @pl.when(k > 0)
            def _():
                r3s[k, at, :] = total
                r3_copy(k, q).start()

    dispatch(z, xin.at[z, mine])
    pl.semaphore_wait(barrier, experts + 1)

    @pl.loop(0, nq)
    def _(q):
        forward_z(0, q)

    @pl.loop(1, experts)
    def _(k):
        dispatch(peer(k), disp.at[k])

        @pl.loop(0, nq)
        def _(q):
            z_copy(k, q).start()

    acc[...] = jnp.zeros_like(acc)

    def gate_up(k, j):
        @pl.when(k == 0)
        def _():
            for copy in weight_gu(j):
                copy.wait()

        cols = pl.ds(pl.multiple_of(j * ft, ft), ft)
        inputs = xin[peer(k)].reshape(SPLIT * cap, width)
        gate = jnp.dot(inputs, wg[:, cols], preferred_element_type=f32)
        up = jnp.dot(inputs, wu[:, cols], preferred_element_type=f32)
        hid[:, cols] = (gate / (1.0 + jnp.exp(-gate)) * up).astype(bf16)

    def down(k, j):
        cols = pl.ds(pl.multiple_of(j * dt, dt), dt)
        res = jnp.dot(hid[...], wd[:, cols], preferred_element_type=f32).astype(bf16)
        part[k, :, :, :, cols] = res.reshape(2, 2, cap, dt)

    early = 0

    @pl.loop(0, nq)
    def _(q):
        forward_y(0, q)

        @pl.when(q < early)
        def _():
            forward_z(1, q)

    @pl.loop(0, experts)
    def _(k):
        @pl.loop(0, nq)
        def _(q):
            c_arrival(k, q).wait_recv()

        @pl.loop(0, nq)
        def _(q):
            d_arrival(k, q).wait_recv()

        @pl.loop(0, max(nf, nq))
        def _(j):
            @pl.when(j < nf)
            def _():
                gate_up(k, j)

            @pl.when((j < nq) & (k + 1 < experts) & ((k > 0) | (j >= early)))
            def _():
                forward_z(k + 1, j)

            @pl.when((j < nq) & (k > 0))
            def _():
                reduce_chip(k - 1, j)

        @pl.when(k == 0)
        def _():
            weight_d.wait()

        @pl.loop(0, max(nd, nq))
        def _(j):
            @pl.when(j < nd)
            def _():
                down(k, j)

            @pl.when((j < nq) & (k + 1 < experts))
            def _():
                forward_y(k + 1, j)

            @pl.when((j < nq) & (k > 0))
            def _():
                reduce_group(k - 1, j)

        for side in (1 - y, y):

            @pl.loop(0, nq)
            def _(q):
                r1_copy(k, side, q).start()

    @pl.loop(0, nq)
    def _(q):
        reduce_chip(experts - 1, q)

    @pl.loop(0, nq)
    def _(q):
        reduce_group(experts - 1, q)

    @pl.loop(0, experts)
    def _(k):
        e = peer(k)

        @pl.when(k > 0)
        def _():
            @pl.loop(0, nq)
            def _(q):
                r3_arrival(k, q).wait_recv()

        slot = jnp.sum(jnp.where(lane == e, rank, 0.0), axis=1, keepdims=True)
        weight = jnp.sum(jnp.where(lane == e, weight_c, 0.0), axis=1, keepdims=True)
        place = lax.broadcasted_iota(jnp.int32, (rows, cap), 1)
        pick = (place == slot.astype(jnp.int32)).astype(f32).astype(bf16)
        wide = tile_of(width, 512)
        for n in range(width // wide):
            cols = slice(n * wide, (n + 1) * wide)
            acc[:, cols] += weight * jnp.dot(pick, home[e, :, cols], preferred_element_type=f32)

    out_ref[...] = acc[...].astype(bf16)

    @pl.loop(0, experts)
    def _(k):
        @pl.when(k > 0)
        def _():
            @pl.loop(0, nq)
            def _(q):
                z_copy(k, q).wait_send()

            @pl.loop(0, nq)
            def _(q):
                r3_copy(k, q).wait_send()

        @pl.loop(0, nq)
        def _(q):
            y_copy(k, q).wait_send()
            c_copy(k, q).wait_send()

        @pl.loop(0, nq)
        def _(q):
            d_copy(k, q).wait_send()
            r2_copy(k, q).wait_send()

        for v in range(2):
            @pl.loop(0, nq)
            def _(q):
                r1_copy(k, v, q).wait_send()


def local(tokens, norm_gain, expert_ids, mix_weights, gate_weight, up_weight, down_weight):
    n_dev = lax.axis_size("ep")
    experts = n_dev // SPLIT
    rows, width = tokens.shape
    top = expert_ids.shape[1]
    ff = gate_weight.shape[1]
    cap = (rows * top * SPLIT * 5 + 4 * n_dev - 1) // (4 * n_dev)
    cap = (cap + CHUNK - 1) // CHUNK * CHUNK
    nq = cap // CHUNK
    nf = ff // tile_of(ff, 256)
    dma = pltpu.SemaphoreType.DMA
    vmem = pl.BlockSpec(memory_space=pltpu.VMEM)
    hbm = pl.BlockSpec(memory_space=pl.ANY)
    block = (cap, width)
    return pl.pallas_call(
        functools.partial(kernel, experts),
        out_shape=jax.ShapeDtypeStruct((rows, width), bf16),
        in_specs=[vmem, vmem, vmem, vmem, hbm, hbm, hbm],
        out_specs=vmem,
        scratch_shapes=[
            pltpu.VMEM((width, ff), bf16),
            pltpu.VMEM((width, ff), bf16),
            pltpu.VMEM((ff, width), bf16),
            pltpu.VMEM((rows, width), bf16),
            pltpu.VMEM((experts,) + block, bf16),
            pltpu.VMEM((experts, SPLIT) + block, bf16),
            pltpu.VMEM((SPLIT * cap, ff), bf16),
            pltpu.VMEM((experts, 2, 2) + block, bf16),
            pltpu.VMEM((experts, 2) + block, bf16),
            pltpu.VMEM((experts,) + block, bf16),
            pltpu.VMEM((experts,) + block, bf16),
            pltpu.VMEM((experts,) + block, bf16),
            pltpu.VMEM((experts,) + block, bf16),
            pltpu.VMEM((rows, width), f32),
            dma((3, nf)),
        ] + [dma((experts, nq))] * 8 + [dma((experts, 2, nq))] * 2 + [dma((experts, nq))] * 4,
        compiler_params=pltpu.CompilerParams(
            collective_id=0, has_side_effects=True, vmem_limit_bytes=64 * 1024 * 1024 - 65536,
        ),
    )(tokens, norm_gain.reshape(1, width), expert_ids.T, mix_weights.T, gate_weight, up_weight, down_weight)


def solution(mesh):
    in_specs = (
        P(("grp", "ep"), None),
        P(),
        P(("grp", "ep"), None),
        P(("grp", "ep"), None),
        P(None, "ep"),
        P(None, "ep"),
        P("ep", None),
    )
    out_specs = P(("grp", "ep"), None)
    return jax.shard_map(local, mesh=mesh, in_specs=in_specs, out_specs=out_specs, check_vma=False)
```

profile of v0, /device:TPU:0, one launch (start us, length us, event | category | flops | bytes accessed | tf_op | source)
XLA Modules:
  0.0 103.2 jit_solution(1164775939109776207)
XLA Ops:
  0.0 101.3 %shard_map.73 = bf16[128,2048]{1,0:T(8,128)(2,1)} custom-call(bf16[128,2048]{1,0:T(8,128)(2,1)} %tok_ref.1, f32[1,2048]{1,0:T(1,128)} %bitcast.3, s32[2,128]{1,0:T(2,128)} %bitcast.4, f32[2,128]{1,0:T(2,128)} %bitcast.5, bf16[2048,1792]{1,0:T(8,128)(2,1)} %wg_hbm.1, bf16[2048,1792]{1,0:T(8,128)(2,1)} %wu_hbm.1, bf16[1792,2048]{1,0:T(8,128)(2,1)} %wd_hbm.1), custom_call_target="tpu_custom_call" | custom-call | tf_op jit(solution)/shard_map/pallas_call | solution.py:360
  101.3 1.9 %copy.9 = bf16[128,2048]{1,0:T(8,128)(2,1)} copy(bf16[128,2048]{1,0:T(8,128)(2,1)} %shard_map.73) | data formatting | bytes 1048576
where the time goes:
time: 103 us
  Pallas kernels  101 us (98%)
  local copies, waits for them, and re-layouts  1.88 us (2%)
    pallas_call x1, Pallas kernels, local(): pl.pallas_call(functools.partial(kernel, experts), out_shape=jax.ShapeDty...  101 us

commit v1 on v0

--- a/solution.py
+++ b/solution.py
@@ -17,6 +17,72 @@
     while extent % tile:
         tile //= 2
     return tile
+
+
+def cut(extent):
+    first = (extent // 256 + 1) // 2 * 256
+    return ((0, first), (first, extent - first))
+
+
+def plan(experts, nq):
+    last = experts - 1
+    sides = []
+    for inner in (False, True):
+        ev = {}
+
+        def at(step, place, *items, ev=ev):
+            ev.setdefault((step, place), []).extend(items)
+
+        if experts == 4:
+            half = (nq + 1) // 2
+            if inner:
+                at(0, 1, ("z", 2, 0, nq))
+                at(0, 2, ("y", 1, 0, nq - 1))
+                at(0, 3, ("y", 1, nq - 1, nq))
+                at(0, 4, ("z", 3, 0, half - 1))
+                at(1, 1, ("z", 3, half - 1, half))
+                at(1, 2, ("z", 3, half, half + 1))
+                at(1, 3, ("z", 3, half + 1, nq), ("y", 2, 0, nq))
+                at(2, 1, ("chip", 1, 0, nq))
+                at(2, 3, ("y", 3, 0, nq))
+                at(3, 1, ("group", 1, 0, half), ("chip", 0, 0, half))
+                at(3, 2, ("group", 1, half, nq))
+                tail = [
+                    ("chip", 3, 0, nq), ("chip", 2, 0, nq), ("chip", 0, half, nq),
+                    ("group", 0, 0, half), ("group", 3, 0, nq), ("mix", 1), ("group", 2, 0, nq),
+                    ("mix", 2), ("group", 0, half, nq), ("mix", 0), ("mix", 3),
+                ]
+            else:
+                at(0, 1, ("z", 2, 0, 1))
+                at(0, 2, ("z", 2, 1, 2), ("y", 1, 0, nq - 1))
+                at(0, 3, ("y", 1, nq - 1, nq))
+                at(0, 4, ("z", 2, 2, half))
+                at(1, 1, ("z", 2, half, half + 1))
+                at(1, 3, ("z", 2, half + 1, nq))
+                at(1, 4, ("z", 3, 0, 1), ("y", 2, 0, nq))
+                at(2, 1, ("z", 3, 1, half))
+                at(2, 2, ("z", 3, half, nq))
+                at(2, 3, ("chip", 0, 0, half))
+                at(2, 4, ("y", 3, 0, nq))
+                at(3, 1, ("chip", 2, 0, nq))
+                at(3, 2, ("group", 0, 0, half))
+                tail = [
+                    ("chip", 3, 0, nq), ("chip", 1, 0, nq), ("chip", 0, half, nq),
+                    ("group", 2, 0, nq), ("group", 3, 0, nq), ("mix", 1), ("group", 1, 0, nq),
+                    ("mix", 2), ("group", 0, half, nq), ("mix", 0), ("mix", 3),
+                ]
+        else:
+            for k in range(experts):
+                if k + 2 < experts:
+                    at(k, 2, ("z", k + 2, 0, nq))
+                if k + 1 < experts:
+                    at(k, 4, ("y", k + 1, 0, nq))
+                if k > 0:
+                    at(k, 1, ("chip", k - 1, 0, nq))
+                    at(k, 3, ("group", k - 1, 0, nq))
+            tail = [("chip", last, 0, nq), ("group", last, 0, nq)] + [("mix", k) for k in range(experts)]
+        sides.append((ev, tail))
+    return sides
 
 
 def kernel(
@@ -42,10 +108,14 @@
     other_y = c * 2 + 1 - y
     other_c = (1 - c) * 2 + y
     other_yc = (1 - c) * 2 + 1 - y
+    near = jnp.minimum(z, experts - 1 - z)
+    away = jnp.where(2 * z < experts, 1, -1)
+    inner = near > 0
+    edge = near == 0
 
     def peer(k):
-        shift = jnp.where(k == 0, 0, (k + experts // 2 - 2) % (experts - 1) + 1)
-        return z ^ shift
+        both = z + away * ((k + 1) // 2) * (2 * (k % 2) - 1)
+        return jnp.where(k <= 2 * near, both, z + away * (k - near))
 
     def at_z(k):
         return {"ep": peer(k) * SPLIT + y * 2 + c}
@@ -59,33 +129,31 @@
     def chunk(q):
         return pl.ds(pl.multiple_of(q * CHUNK, CHUNK), CHUNK)
 
-    ft = tile_of(ff, 256)
-    nf = ff // ft
-    dt = tile_of(width, 256)
-    nd = width // dt
-
-    def weight_gu(j):
-        cols = pl.ds(pl.multiple_of(j * ft, ft), ft)
-        return (
-            pltpu.make_async_copy(wg_hbm.at[:, cols], wg.at[:, cols], w_sem.at[0, j]),
-            pltpu.make_async_copy(wu_hbm.at[:, cols], wu.at[:, cols], w_sem.at[1, j]),
-        )
-
-    weight_d = pltpu.make_async_copy(wd_hbm, wd, w_sem.at[2, 0])
+    ff_cuts = cut(ff)
+    out_cuts = cut(width)
+    pieces = w_sem.shape[1]
+
+    def weight(which):
+        hbm, vmem = ((wg_hbm, wg), (wu_hbm, wu), (wd_hbm, wd))[which]
+        size = hbm.shape[0] // pieces
+        return [
+            pltpu.make_async_copy(
+                hbm.at[pl.ds(i * size, size)], vmem.at[pl.ds(i * size, size)], w_sem.at[which, i]
+            )
+            for i in range(pieces)
+        ]
 
     barrier = pltpu.get_barrier_semaphore()
-
     for k in range(1, experts):
         pl.semaphore_signal(barrier, inc=1, device_id=at_z(k), device_id_type=pl.DeviceIdType.MESH)
     pl.semaphore_signal(barrier, inc=1, device_id=at_y, device_id_type=pl.DeviceIdType.MESH)
     pl.semaphore_signal(barrier, inc=1, device_id=at_c, device_id_type=pl.DeviceIdType.MESH)
 
-    for j in range(nf):
-        for copy in weight_gu(j):
+    for which in range(3):
+        for copy in weight(which):
             copy.start()
-    weight_d.start()
-
-    step = tile_of(rows, 16)
+
+    step = tile_of(rows, 32)
 
     @pl.loop(0, rows // step)
     def _(r):
@@ -142,9 +210,11 @@
     d_copy = in_group(other_y, ds_sem, dr_sem, at_c)
     d_arrival = in_group(other_yc, ds_sem, dr_sem, at_c)
 
-    def r1_copy(k, v, q):
+    def r1_copy(k, v, h):
+        start, size = out_cuts[h]
+        cols = pl.ds(start, size)
         return remote(
-            part.at[k, 1 - c, v, chunk(q)], r1.at[k, v, chunk(q)], r1s_sem.at[k, v, q], r1r_sem.at[k, v, q], at_c
+            part.at[k, 1 - c, v, :, cols], r1.at[k, v, :, cols], r1s_sem.at[k, v, h], r1r_sem.at[k, v, h], at_c
         )
 
     def r2_copy(k, q):
@@ -158,10 +228,8 @@
         return remote(r3s.at[k, chunk(q)], home.at[p, chunk(q)], r3s_sem.at[k, q], r3r_sem.at[p, q], at_z(k))
 
     def forward_z(k, q):
-        @pl.when(k > 0)
-        def _():
+        if k > 0:
             z_arrival(k, q).wait_recv()
-
         y_copy(k, q).start()
         c_copy(k, q).start()
 
@@ -169,30 +237,79 @@
         y_arrival(k, q).wait_recv()
         d_copy(k, q).start()
 
-    def reduce_chip(k, q):
+    def chip_sum(k, q):
         at = chunk(q)
-        r1_copy(k, 1 - y, q).wait_recv()
+
+        @pl.when(q == 0)
+        def _():
+            for h in range(2):
+                r1_copy(k, 1 - y, h).wait_recv()
+
         r2s[k, at, :] = (part[k, c, 1 - y, at, :].astype(f32) + r1[k, 1 - y, at, :].astype(f32)).astype(bf16)
         r2_copy(k, q).start()
 
-    def reduce_group(k, q):
-        @pl.when(q < nq)
+    def group_sum(k, q):
+        at = chunk(q)
+
+        @pl.when(q == 0)
         def _():
-            at = chunk(q)
-            r1_copy(k, y, q).wait_recv()
-            r2_copy(k, q).wait_recv()
-            total = (
-                part[k, c, y, at, :].astype(f32) + r1[k, y, at, :].astype(f32) + r2r[k, at, :].astype(f32)
-            ).astype(bf16)
-
-            @pl.when(k == 0)
-            def _():
-                home[z, at, :] = total
-
-            @pl.when(k > 0)
-            def _():
-                r3s[k, at, :] = total
-                r3_copy(k, q).start()
+            for h in range(2):
+                r1_copy(k, y, h).wait_recv()
+
+        r2_copy(k, q).wait_recv()
+        total = (
+            part[k, c, y, at, :].astype(f32) + r1[k, y, at, :].astype(f32) + r2r[k, at, :].astype(f32)
+        ).astype(bf16)
+        if k == 0:
+            home[z, at, :] = total
+        else:
+            r3s[k, at, :] = total
+            r3_copy(k, q).start()
+
+    def mix(k):
+        e = peer(k)
+        if k > 0:
+            @pl.loop(0, nq)
+            def _(q):
+                r3_arrival(k, q).wait_recv()
+
+        slot = jnp.sum(jnp.where(lane == e, rank, 0.0), axis=1, keepdims=True)
+        share = jnp.sum(jnp.where(lane == e, weight_c, 0.0), axis=1, keepdims=True)
+        place = lax.broadcasted_iota(jnp.int32, (rows, cap), 1)
+        pick = (place == slot.astype(jnp.int32)).astype(f32).astype(bf16)
+        wide = tile_of(width, 512)
+        for n in range(width // wide):
+            cols = slice(n * wide, (n + 1) * wide)
+            acc[:, cols] += share * jnp.dot(pick, home[e, :, cols], preferred_element_type=f32)
+
+    actions = {"z": forward_z, "y": forward_y, "chip": chip_sum, "group": group_sum}
+    sides = plan(experts, nq)
+
+    def perform(items):
+        for item in items:
+            if item[0] == "mix":
+                mix(item[1])
+            else:
+                kind, k, lo, hi = item
+
+                @pl.loop(lo, hi)
+                def _(q):
+                    actions[kind](k, q)
+
+    def service(step_index, place):
+        for k in range(experts):
+            lists = [side[0].get((k, place), []) for side in sides]
+            if lists[0] == lists[1]:
+                if lists[0]:
+                    @pl.when(step_index == k)
+                    def _():
+                        perform(lists[0])
+            else:
+                for items, kind in zip(lists, (edge, inner)):
+                    if items:
+                        @pl.when((step_index == k) & kind)
+                        def _():
+                            perform(items)
 
     dispatch(z, xin.at[z, mine])
     pl.semaphore_wait(barrier, experts + 1)
@@ -211,107 +328,47 @@
 
     acc[...] = jnp.zeros_like(acc)
 
-    def gate_up(k, j):
-        @pl.when(k == 0)
-        def _():
-            for copy in weight_gu(j):
-                copy.wait()
-
-        cols = pl.ds(pl.multiple_of(j * ft, ft), ft)
-        inputs = xin[peer(k)].reshape(SPLIT * cap, width)
-        gate = jnp.dot(inputs, wg[:, cols], preferred_element_type=f32)
-        up = jnp.dot(inputs, wu[:, cols], preferred_element_type=f32)
-        hid[:, cols] = (gate / (1.0 + jnp.exp(-gate)) * up).astype(bf16)
-
-    def down(k, j):
-        cols = pl.ds(pl.multiple_of(j * dt, dt), dt)
-        res = jnp.dot(hid[...], wd[:, cols], preferred_element_type=f32).astype(bf16)
-        part[k, :, :, :, cols] = res.reshape(2, 2, cap, dt)
-
-    early = 0
-
     @pl.loop(0, nq)
     def _(q):
         forward_y(0, q)
-
-        @pl.when(q < early)
-        def _():
+        if experts > 1:
             forward_z(1, q)
+
+    for which in range(3):
+        for copy in weight(which):
+            copy.wait()
 
     @pl.loop(0, experts)
     def _(k):
         @pl.loop(0, nq)
         def _(q):
             c_arrival(k, q).wait_recv()
-
-        @pl.loop(0, nq)
-        def _(q):
             d_arrival(k, q).wait_recv()
 
-        @pl.loop(0, max(nf, nq))
-        def _(j):
-            @pl.when(j < nf)
+        for h, (start, size) in enumerate(ff_cuts):
+            cols = slice(start, start + size)
+            inputs = xin[peer(k)].reshape(SPLIT * cap, width)
+            gate = jnp.dot(inputs, wg[:, cols], preferred_element_type=f32)
+            up = jnp.dot(inputs, wu[:, cols], preferred_element_type=f32)
+            hid[:, cols] = (gate / (1.0 + jnp.exp(-gate)) * up).astype(bf16)
+            service(k, 1 + h)
+
+        for h, (start, size) in enumerate(out_cuts):
+            cols = slice(start, start + size)
+            res = jnp.dot(hid[...], wd[:, cols], preferred_element_type=f32).astype(bf16)
+            part[k, :, :, :, cols] = res.reshape(2, 2, cap, size)
+            for v in (1 - y, y):
+                r1_copy(k, v, h).start()
+            service(k, 3 + h)
+
+    tails = [side[1] for side in sides]
+    if tails[0] == tails[1]:
+        perform(tails[0])
+    else:
+        for items, kind in zip(tails, (edge, inner)):
+            @pl.when(kind)
             def _():
-                gate_up(k, j)
-
-            @pl.when((j < nq) & (k + 1 < experts) & ((k > 0) | (j >= early)))
-            def _():
-                forward_z(k + 1, j)
-
-            @pl.when((j < nq) & (k > 0))
-            def _():
-                reduce_chip(k - 1, j)
-
-        @pl.when(k == 0)
-        def _():
-            weight_d.wait()
-
-        @pl.loop(0, max(nd, nq))
-        def _(j):
-            @pl.when(j < nd)
-            def _():
-                down(k, j)
-
-            @pl.when((j < nq) & (k + 1 < experts))
-            def _():
-                forward_y(k + 1, j)
-
-            @pl.when((j < nq) & (k > 0))
-            def _():
-                reduce_group(k - 1, j)
-
-        for side in (1 - y, y):
-
-            @pl.loop(0, nq)
-            def _(q):
-                r1_copy(k, side, q).start()
-
-    @pl.loop(0, nq)
-    def _(q):
-        reduce_chip(experts - 1, q)
-
-    @pl.loop(0, nq)
-    def _(q):
-        reduce_group(experts - 1, q)
-
-    @pl.loop(0, experts)
-    def _(k):
-        e = peer(k)
-
-        @pl.when(k > 0)
-        def _():
-            @pl.loop(0, nq)
-            def _(q):
-                r3_arrival(k, q).wait_recv()
-
-        slot = jnp.sum(jnp.where(lane == e, rank, 0.0), axis=1, keepdims=True)
-        weight = jnp.sum(jnp.where(lane == e, weight_c, 0.0), axis=1, keepdims=True)
-        place = lax.broadcasted_iota(jnp.int32, (rows, cap), 1)
-        pick = (place == slot.astype(jnp.int32)).astype(f32).astype(bf16)
-        wide = tile_of(width, 512)
-        for n in range(width // wide):
-            cols = slice(n * wide, (n + 1) * wide)
-            acc[:, cols] += weight * jnp.dot(pick, home[e, :, cols], preferred_element_type=f32)
+                perform(items)
 
     out_ref[...] = acc[...].astype(bf16)
 
@@ -322,25 +379,18 @@
             @pl.loop(0, nq)
             def _(q):
                 z_copy(k, q).wait_send()
-
-            @pl.loop(0, nq)
-            def _(q):
                 r3_copy(k, q).wait_send()
 
         @pl.loop(0, nq)
         def _(q):
             y_copy(k, q).wait_send()
             c_copy(k, q).wait_send()
-
-        @pl.loop(0, nq)
-        def _(q):
             d_copy(k, q).wait_send()
             r2_copy(k, q).wait_send()
 
         for v in range(2):
-            @pl.loop(0, nq)
-            def _(q):
-                r1_copy(k, v, q).wait_send()
+            for h in range(2):
+                r1_copy(k, v, h).wait_send()
 
 
 def local(tokens, norm_gain, expert_ids, mix_weights, gate_weight, up_weight, down_weight):
@@ -352,7 +402,6 @@
     cap = (rows * top * SPLIT * 5 + 4 * n_dev - 1) // (4 * n_dev)
     cap = (cap + CHUNK - 1) // CHUNK * CHUNK
     nq = cap // CHUNK
-    nf = ff // tile_of(ff, 256)
     dma = pltpu.SemaphoreType.DMA
     vmem = pl.BlockSpec(memory_space=pltpu.VMEM)
     hbm = pl.BlockSpec(memory_space=pl.ANY)
@@ -377,8 +426,8 @@
             pltpu.VMEM((experts,) + block, bf16),
             pltpu.VMEM((experts,) + block, bf16),
             pltpu.VMEM((rows, width), f32),
-            dma((3, nf)),
-        ] + [dma((experts, nq))] * 8 + [dma((experts, 2, nq))] * 2 + [dma((experts, nq))] * 4,
+            dma((3, 4)),
+        ] + [dma((experts, nq))] * 8 + [dma((experts, 2, 2))] * 2 + [dma((experts, nq))] * 4,
         compiler_params=pltpu.CompilerParams(
             collective_id=0, has_side_effects=True, vmem_limit_bytes=64 * 1024 * 1024 - 65536,
         ),

time: 103 us -> 111 us (1.078); the launches traced: 103 us -> 110 us
  Pallas kernels: 101 us -> 108 us
    pallas_call x1, Pallas kernels: 101 us -> 108 us  [local(): pl.pallas_call(functools.partial(kernel, experts), out_shape=jax.ShapeDty...]
where the time goes in v1:
time: 111 us; the launch traced here: 110 us
  Pallas kernels  108 us (97%)
  local copies, waits for them, and re-layouts  1.88 us (2%)
    pallas_call x1, Pallas kernels, local(): pl.pallas_call(functools.partial(kernel, experts), out_shape=jax.ShapeDty...  108 us

profile of v1, /device:TPU:0, one launch (start us, length us, event | category | flops | bytes accessed | tf_op | source)
XLA Modules:
  0.0 109.9 jit_solution(3080934670791075927)
XLA Ops:
  0.0 108.0 %shard_map.73 = bf16[128,2048]{1,0:T(8,128)(2,1)} custom-call(bf16[128,2048]{1,0:T(8,128)(2,1)} %tok_ref.1, f32[1,2048]{1,0:T(1,128)} %bitcast.3, s32[2,128]{1,0:T(2,128)} %bitcast.4, f32[2,128]{1,0:T(2,128)} %bitcast.5, bf16[2048,1792]{1,0:T(8,128)(2,1)} %wg_hbm.1, bf16[2048,1792]{1,0:T(8,128)(2,1)} %wu_hbm.1, bf16[1792,2048]{1,0:T(8,128)(2,1)} %wd_hbm.1), custom_call_target="tpu_custom_call" | custom-call | tf_op jit(solution)/shard_map/pallas_call | solution.py:409
  108.0 1.9 %copy.9 = bf16[128,2048]{1,0:T(8,128)(2,1)} copy(bf16[128,2048]{1,0:T(8,128)(2,1)} %shard_map.73) | data formatting | bytes 1048576

commit v2 on v1

--- a/solution.py
+++ b/solution.py
@@ -19,9 +19,10 @@
     return tile
 
 
-def cut(extent):
-    first = (extent // 256 + 1) // 2 * 256
-    return ((0, first), (first, extent - first))
+def cut(extent, parts):
+    tiles = extent // 256
+    ends = [tiles * i // parts * 256 for i in range(parts)] + [extent]
+    return tuple((a, b - a) for a, b in zip(ends, ends[1:]))
 
 
 def plan(experts, nq):
@@ -31,56 +32,65 @@
         ev = {}
 
         def at(step, place, *items, ev=ev):
-            ev.setdefault((step, place), []).extend(items)
+            ev.setdefault((step, place), []).extend(
+                (kind, k, nq * lo // 5, nq * hi // 5) for kind, k, lo, hi in items
+            )
 
         if experts == 4:
-            half = (nq + 1) // 2
             if inner:
-                at(0, 1, ("z", 2, 0, nq))
-                at(0, 2, ("y", 1, 0, nq - 1))
-                at(0, 3, ("y", 1, nq - 1, nq))
-                at(0, 4, ("z", 3, 0, half - 1))
-                at(1, 1, ("z", 3, half - 1, half))
-                at(1, 2, ("z", 3, half, half + 1))
-                at(1, 3, ("z", 3, half + 1, nq), ("y", 2, 0, nq))
-                at(2, 1, ("chip", 1, 0, nq))
-                at(2, 3, ("y", 3, 0, nq))
-                at(3, 1, ("group", 1, 0, half), ("chip", 0, 0, half))
-                at(3, 2, ("group", 1, half, nq))
-                tail = [
-                    ("chip", 3, 0, nq), ("chip", 2, 0, nq), ("chip", 0, half, nq),
-                    ("group", 0, 0, half), ("group", 3, 0, nq), ("mix", 1), ("group", 2, 0, nq),
-                    ("mix", 2), ("group", 0, half, nq), ("mix", 0), ("mix", 3),
-                ]
+                at(0, 1, ("z", 2, 0, 5))
+                at(0, 3, ("y", 1, 0, 4))
+                at(0, 4, ("y", 1, 4, 5))
+                at(1, 1, ("chip", 0, 0, 2))
+                at(1, 2, ("z", 3, 0, 2))
+                at(1, 3, ("z", 3, 2, 3), ("y", 2, 0, 5))
+                at(1, 4, ("z", 3, 3, 4))
+                at(1, 5, ("z", 3, 4, 5))
+                at(2, 1, ("chip", 1, 0, 5), ("y", 3, 0, 2))
+                at(2, 3, ("y", 3, 2, 4))
+                at(2, 4, ("y", 3, 4, 5))
+                at(2, 5, ("group", 1, 0, 2))
+                at(3, 1, ("chip", 2, 0, 5), ("group", 1, 2, 3))
+                at(3, 2, ("group", 1, 3, 4))
+                at(3, 3, ("group", 1, 4, 5))
+                at(3, 5, ("group", 2, 0, 2))
+                at(4, 0, ("chip", 3, 0, 5), ("chip", 0, 2, 5), ("group", 2, 2, 5), ("group", 3, 0, 5))
+                at(4, 0, ("mix", 1, 0, 5), ("group", 0, 0, 5))
+                at(4, 0, ("mix", 0, 0, 5), ("mix", 2, 0, 5), ("mix", 3, 0, 5))
             else:
-                at(0, 1, ("z", 2, 0, 1))
-                at(0, 2, ("z", 2, 1, 2), ("y", 1, 0, nq - 1))
-                at(0, 3, ("y", 1, nq - 1, nq))
-                at(0, 4, ("z", 2, 2, half))
-                at(1, 1, ("z", 2, half, half + 1))
-                at(1, 3, ("z", 2, half + 1, nq))
-                at(1, 4, ("z", 3, 0, 1), ("y", 2, 0, nq))
-                at(2, 1, ("z", 3, 1, half))
-                at(2, 2, ("z", 3, half, nq))
-                at(2, 3, ("chip", 0, 0, half))
-                at(2, 4, ("y", 3, 0, nq))
-                at(3, 1, ("chip", 2, 0, nq))
-                at(3, 2, ("group", 0, 0, half))
-                tail = [
-                    ("chip", 3, 0, nq), ("chip", 1, 0, nq), ("chip", 0, half, nq),
-                    ("group", 2, 0, nq), ("group", 3, 0, nq), ("mix", 1), ("group", 1, 0, nq),
-                    ("mix", 2), ("group", 0, half, nq), ("mix", 0), ("mix", 3),
-                ]
+                at(0, 2, ("z", 2, 0, 1))
+                at(0, 3, ("z", 2, 1, 2), ("y", 1, 0, 4))
+                at(0, 4, ("y", 1, 4, 5), ("z", 2, 2, 4))
+                at(0, 5, ("z", 2, 4, 5))
+                at(1, 1, ("chip", 0, 0, 2))
+                at(1, 4, ("y", 2, 0, 5))
+                at(1, 5, ("z", 3, 0, 1))
+                at(2, 1, ("z", 3, 1, 2))
+                at(2, 2, ("z", 3, 2, 4))
+                at(2, 3, ("z", 3, 4, 5), ("chip", 1, 0, 2))
+                at(2, 4, ("y", 3, 0, 3))
+                at(2, 5, ("y", 3, 3, 5), ("chip", 1, 2, 3))
+                at(3, 1, ("chip", 2, 0, 5))
+                at(3, 2, ("group", 1, 0, 2))
+                at(3, 3, ("group", 2, 0, 1))
+                at(3, 4, ("group", 2, 1, 2))
+                at(3, 5, ("group", 2, 2, 3))
+                at(4, 0, ("chip", 3, 0, 5), ("chip", 1, 3, 5), ("chip", 0, 2, 5), ("group", 2, 3, 5))
+                at(4, 0, ("group", 1, 2, 3), ("group", 0, 0, 2), ("group", 3, 0, 5), ("mix", 2, 0, 5))
+                at(4, 0, ("group", 1, 3, 5), ("group", 0, 2, 5))
+                at(4, 0, ("mix", 0, 0, 5), ("mix", 1, 0, 5), ("mix", 3, 0, 5))
         else:
             for k in range(experts):
                 if k + 2 < experts:
-                    at(k, 2, ("z", k + 2, 0, nq))
+                    at(k, 2, ("z", k + 2, 0, 5))
                 if k + 1 < experts:
-                    at(k, 4, ("y", k + 1, 0, nq))
+                    at(k, 5, ("y", k + 1, 0, 5))
                 if k > 0:
-                    at(k, 1, ("chip", k - 1, 0, nq))
-                    at(k, 3, ("group", k - 1, 0, nq))
-            tail = [("chip", last, 0, nq), ("group", last, 0, nq)] + [("mix", k) for k in range(experts)]
+                    at(k, 1, ("chip", k - 1, 0, 5))
+                    at(k, 3, ("group", k - 1, 0, 5))
+            at(experts, 0, ("chip", last, 0, 5), ("group", last, 0, 5))
+            at(experts, 0, *[("mix", k, 0, 5) for k in range(experts)])
+        tail = ev.pop((experts, 0))
         sides.append((ev, tail))
     return sides
 
@@ -115,7 +125,9 @@
 
     def peer(k):
         both = z + away * ((k + 1) // 2) * (2 * (k % 2) - 1)
-        return jnp.where(k <= 2 * near, both, z + away * (k - near))
+        from_edge = z + away * jnp.where(k < 2, k, experts + 1 - k)
+        from_inner = jnp.where(k <= 2 * near, both, z + away * (k - near))
+        return jnp.where(edge, from_edge, from_inner)
 
     def at_z(k):
         return {"ep": peer(k) * SPLIT + y * 2 + c}
@@ -129,8 +141,8 @@
     def chunk(q):
         return pl.ds(pl.multiple_of(q * CHUNK, CHUNK), CHUNK)
 
-    ff_cuts = cut(ff)
-    out_cuts = cut(width)
+    ff_cuts = cut(ff, 3)
+    out_cuts = cut(width, 2)
     pieces = w_sem.shape[1]
 
     def weight(which):
@@ -196,6 +208,11 @@
         p = peer(k)
         return remote(disp.at[k, chunk(q)], xin.at[p, mine, chunk(q)], zs_sem.at[k, q], zr_sem.at[p, q], at_z(k))
 
+    def send_z(k):
+        @pl.loop(0, nq)
+        def _(q):
+            z_copy(k, q).start()
+
     def in_group(sub, send, recv, where):
         def make(k, q):
             slot = xin.at[peer(k), sub, chunk(q)]
@@ -322,9 +339,9 @@
     def _(k):
         dispatch(peer(k), disp.at[k])
 
-        @pl.loop(0, nq)
-        def _(q):
-            z_copy(k, q).start()
+        @pl.when((k == 1) | (inner & (k == 2)))
+        def _():
+            send_z(k)
 
     acc[...] = jnp.zeros_like(acc)
 
@@ -333,6 +350,12 @@
         forward_y(0, q)
         if experts > 1:
             forward_z(1, q)
+
+    @pl.loop(2, experts)
+    def _(k):
+        @pl.when(edge | (k > 2))
+        def _():
+            send_z(k)
 
     for which in range(3):
         for copy in weight(which):
@@ -359,7 +382,7 @@
             part[k, :, :, :, cols] = res.reshape(2, 2, cap, size)
             for v in (1 - y, y):
                 r1_copy(k, v, h).start()
-            service(k, 3 + h)
+            service(k, 1 + len(ff_cuts) + h)
 
     tails = [side[1] for side in sides]
     if tails[0] == tails[1]:

time: 111 us -> 81.9 us (0.74)
  Pallas kernels: 108 us -> 79.9 us
    pallas_call x1, Pallas kernels: 108 us -> 79.9 us  [local(): pl.pallas_call(functools.partial(kernel, experts), out_shape=jax.ShapeDty...]
where the time goes in v2:
time: 81.9 us; the launch traced here: 81.8 us
  Pallas kernels  79.9 us (98%)
  local copies, waits for them, and re-layouts  1.88 us (2%)
    pallas_call x1, Pallas kernels, local(): pl.pallas_call(functools.partial(kernel, experts), out_shape=jax.ShapeDty...  79.9 us
    unnamed x1, local copies, waits for them, and re-layouts  1.88 us

profile of v2, /device:TPU:0, one launch (start us, length us, event | category | flops | bytes accessed | tf_op | source)
XLA Modules:
  0.0 81.8 jit_solution(6594698763012260946)
XLA Ops:
  0.0 79.9 %shard_map.73 = bf16[128,2048]{1,0:T(8,128)(2,1)} custom-call(bf16[128,2048]{1,0:T(8,128)(2,1)} %tok_ref.1, f32[1,2048]{1,0:T(1,128)} %bitcast.3, s32[2,128]{1,0:T(2,128)} %bitcast.4, f32[2,128]{1,0:T(2,128)} %bitcast.5, bf16[2048,1792]{1,0:T(8,128)(2,1)} %wg_hbm.1, bf16[2048,1792]{1,0:T(8,128)(2,1)} %wu_hbm.1, bf16[1792,2048]{1,0:T(8,128)(2,1)} %wd_hbm.1), custom_call_target="tpu_custom_call" | custom-call | tf_op jit(solution)/shard_map/pallas_call | solution.py:432
  79.9 1.9 %copy.9 = bf16[128,2048]{1,0:T(8,128)(2,1)} copy(bf16[128,2048]{1,0:T(8,128)(2,1)} %shard_map.73) | data formatting | bytes 1048576

commit v3 on v2

--- a/solution.py
+++ b/solution.py
@@ -38,47 +38,51 @@
 
         if experts == 4:
             if inner:
-                at(0, 1, ("z", 2, 0, 5))
+                at(0, 1, ("z", 3, 0, 2))
                 at(0, 3, ("y", 1, 0, 4))
-                at(0, 4, ("y", 1, 4, 5))
-                at(1, 1, ("chip", 0, 0, 2))
-                at(1, 2, ("z", 3, 0, 2))
-                at(1, 3, ("z", 3, 2, 3), ("y", 2, 0, 5))
-                at(1, 4, ("z", 3, 3, 4))
-                at(1, 5, ("z", 3, 4, 5))
-                at(2, 1, ("chip", 1, 0, 5), ("y", 3, 0, 2))
-                at(2, 3, ("y", 3, 2, 4))
-                at(2, 4, ("y", 3, 4, 5))
-                at(2, 5, ("group", 1, 0, 2))
-                at(3, 1, ("chip", 2, 0, 5), ("group", 1, 2, 3))
-                at(3, 2, ("group", 1, 3, 4))
-                at(3, 3, ("group", 1, 4, 5))
-                at(3, 5, ("group", 2, 0, 2))
-                at(4, 0, ("chip", 3, 0, 5), ("chip", 0, 2, 5), ("group", 2, 2, 5), ("group", 3, 0, 5))
-                at(4, 0, ("mix", 1, 0, 5), ("group", 0, 0, 5))
-                at(4, 0, ("mix", 0, 0, 5), ("mix", 2, 0, 5), ("mix", 3, 0, 5))
+                at(0, 4, ("y", 1, 4, 5), ("z", 3, 2, 4))
+                at(1, 1, ("z", 2, 0, 1))
+                at(1, 2, ("z", 2, 1, 3))
+                at(1, 3, ("z", 2, 3, 4))
+                at(1, 4, ("z", 2, 4, 5))
+                at(1, 5, ("chip", 1, 0, 5), ("y", 2, 0, 3), ("z", 3, 4, 5), ("chip", 1, 5, 10))
+                at(1, 5, ("y", 2, 3, 5))
+                at(2, 1, ("group", 1, 0, 1))
+                at(2, 2, ("group", 1, 1, 4))
+                at(2, 3, ("chip", 0, 0, 3), ("group", 1, 4, 7))
+                at(2, 4, ("y", 3, 0, 5), ("group", 1, 7, 8))
+                at(2, 5, ("chip", 2, 0, 5), ("group", 1, 8, 10), ("chip", 2, 5, 10))
+                at(3, 1, ("group", 2, 0, 1))
+                at(3, 2, ("group", 2, 1, 4))
+                at(3, 3, ("group", 2, 4, 7))
+                at(3, 4, ("chip", 0, 3, 5), ("group", 2, 7, 9))
+                at(3, 5, ("chip", 3, 0, 5), ("group", 2, 9, 10))
+                at(4, 0, ("chip", 3, 5, 10), ("chip", 0, 5, 10), ("group", 0, 0, 5))
+                at(4, 0, ("mix", 1, 0, 5), ("group", 3, 0, 10), ("group", 0, 5, 10))
+                at(4, 0, ("mix", 0, 0, 5), ("mix", 3, 0, 5), ("mix", 2, 0, 5))
             else:
                 at(0, 2, ("z", 2, 0, 1))
                 at(0, 3, ("z", 2, 1, 2), ("y", 1, 0, 4))
                 at(0, 4, ("y", 1, 4, 5), ("z", 2, 2, 4))
                 at(0, 5, ("z", 2, 4, 5))
-                at(1, 1, ("chip", 0, 0, 2))
-                at(1, 4, ("y", 2, 0, 5))
-                at(1, 5, ("z", 3, 0, 1))
-                at(2, 1, ("z", 3, 1, 2))
-                at(2, 2, ("z", 3, 2, 4))
-                at(2, 3, ("z", 3, 4, 5), ("chip", 1, 0, 2))
-                at(2, 4, ("y", 3, 0, 3))
-                at(2, 5, ("y", 3, 3, 5), ("chip", 1, 2, 3))
-                at(3, 1, ("chip", 2, 0, 5))
-                at(3, 2, ("group", 1, 0, 2))
-                at(3, 3, ("group", 2, 0, 1))
-                at(3, 4, ("group", 2, 1, 2))
-                at(3, 5, ("group", 2, 2, 3))
-                at(4, 0, ("chip", 3, 0, 5), ("chip", 1, 3, 5), ("chip", 0, 2, 5), ("group", 2, 3, 5))
-                at(4, 0, ("group", 1, 2, 3), ("group", 0, 0, 2), ("group", 3, 0, 5), ("mix", 2, 0, 5))
-                at(4, 0, ("group", 1, 3, 5), ("group", 0, 2, 5))
-                at(4, 0, ("mix", 0, 0, 5), ("mix", 1, 0, 5), ("mix", 3, 0, 5))
+                at(1, 1, ("chip", 0, 0, 4))
+                at(1, 3, ("chip", 0, 4, 6), ("y", 2, 0, 5))
+                at(1, 4, ("z", 3, 0, 1))
+                at(1, 5, ("z", 3, 1, 2))
+                at(2, 1, ("z", 3, 2, 4))
+                at(2, 2, ("z", 3, 4, 5))
+                at(2, 3, ("chip", 1, 0, 2), ("y", 3, 0, 2))
+                at(2, 4, ("chip", 1, 2, 4), ("y", 3, 2, 5))
+                at(2, 5, ("chip", 2, 0, 10))
+                at(3, 1, ("group", 1, 0, 4))
+                at(3, 2, ("group", 2, 0, 2))
+                at(3, 3, ("group", 2, 2, 5))
+                at(3, 4, ("chip", 1, 4, 7), ("group", 2, 5, 8))
+                at(3, 5, ("chip", 3, 0, 5), ("group", 2, 8, 9))
+                at(4, 0, ("chip", 3, 5, 10), ("chip", 1, 7, 10), ("chip", 0, 6, 10), ("group", 2, 9, 10))
+                at(4, 0, ("group", 1, 4, 7), ("group", 0, 0, 6), ("group", 3, 0, 10), ("mix", 2, 0, 5))
+                at(4, 0, ("group", 1, 7, 10), ("group", 0, 6, 10))
+                at(4, 0, ("mix", 0, 0, 5), ("mix", 3, 0, 5), ("mix", 1, 0, 5))
         else:
             for k in range(experts):
                 if k + 2 < experts:
@@ -86,9 +90,9 @@
                 if k + 1 < experts:
                     at(k, 5, ("y", k + 1, 0, 5))
                 if k > 0:
-                    at(k, 1, ("chip", k - 1, 0, 5))
-                    at(k, 3, ("group", k - 1, 0, 5))
-            at(experts, 0, ("chip", last, 0, 5), ("group", last, 0, 5))
+                    at(k, 1, ("chip", k - 1, 0, 10))
+                    at(k, 3, ("group", k - 1, 0, 10))
+            at(experts, 0, ("chip", last, 0, 10), ("group", last, 0, 10))
             at(experts, 0, *[("mix", k, 0, 5) for k in range(experts)])
         tail = ev.pop((experts, 0))
         sides.append((ev, tail))
@@ -124,9 +128,10 @@
     edge = near == 0
 
     def peer(k):
-        both = z + away * ((k + 1) // 2) * (2 * (k % 2) - 1)
         from_edge = z + away * jnp.where(k < 2, k, experts + 1 - k)
-        from_inner = jnp.where(k <= 2 * near, both, z + away * (k - near))
+        n = jnp.where(k < 2, k, jnp.where(k == experts - 1, 2, k + 1))
+        both = z + away * ((n + 1) // 2) * (2 * (n % 2) - 1)
+        from_inner = jnp.where(n <= 2 * near, both, z + away * (n - near))
         return jnp.where(edge, from_edge, from_inner)
 
     def at_z(k):
@@ -143,14 +148,14 @@
 
     ff_cuts = cut(ff, 3)
     out_cuts = cut(width, 2)
-    pieces = w_sem.shape[1]
+    pieces = 4
 
     def weight(which):
         hbm, vmem = ((wg_hbm, wg), (wu_hbm, wu), (wd_hbm, wd))[which]
         size = hbm.shape[0] // pieces
         return [
             pltpu.make_async_copy(
-                hbm.at[pl.ds(i * size, size)], vmem.at[pl.ds(i * size, size)], w_sem.at[which, i]
+                hbm.at[pl.ds(i * size, size)], vmem.at[pl.ds(i * size, size)], w_sem.at[which]
             )
             for i in range(pieces)
         ]
@@ -202,11 +207,11 @@
             dst[:, cols] = jnp.dot(pick, normed[:, cols], preferred_element_type=f32).astype(bf16)
 
     def z_copy(k, q):
-        return remote(disp.at[k, chunk(q)], xin.at[z, mine, chunk(q)], zs_sem.at[k, q], zr_sem.at[z, q], at_z(k))
+        return remote(disp.at[k, chunk(q)], xin.at[z, mine, chunk(q)], zs_sem, zr_sem.at[z, q], at_z(k))
 
     def z_arrival(k, q):
         p = peer(k)
-        return remote(disp.at[k, chunk(q)], xin.at[p, mine, chunk(q)], zs_sem.at[k, q], zr_sem.at[p, q], at_z(k))
+        return remote(disp.at[k, chunk(q)], xin.at[p, mine, chunk(q)], zs_sem, zr_sem.at[p, q], at_z(k))
 
     def send_z(k):
         @pl.loop(0, nq)
@@ -216,33 +221,45 @@
     def in_group(sub, send, recv, where):
         def make(k, q):
             slot = xin.at[peer(k), sub, chunk(q)]
-            return remote(slot, slot, send.at[k, q], recv.at[k, q], where)
+            return remote(slot, slot, send, recv(k, q), where)
 
         return make
 
-    y_copy = in_group(mine, ys_sem, yr_sem, at_y)
-    y_arrival = in_group(other_y, ys_sem, yr_sem, at_y)
-    c_copy = in_group(mine, cs_sem, cr_sem, at_c)
-    c_arrival = in_group(other_c, cs_sem, cr_sem, at_c)
-    d_copy = in_group(other_y, ds_sem, dr_sem, at_c)
-    d_arrival = in_group(other_yc, ds_sem, dr_sem, at_c)
+    y_copy = in_group(mine, ys_sem, lambda k, q: yr_sem.at[k, q], at_y)
+    y_arrival = in_group(other_y, ys_sem, lambda k, q: yr_sem.at[k, q], at_y)
+    c_copy = in_group(mine, cs_sem, lambda k, q: cr_sem.at[k], at_c)
+    d_copy = in_group(other_y, ds_sem, lambda k, q: dr_sem.at[k], at_c)
+
+    def c_arrival(k):
+        slot = xin.at[peer(k), other_c]
+        return remote(slot, slot, cs_sem, cr_sem.at[k], at_c)
+
+    def d_arrival(k):
+        slot = xin.at[peer(k), other_yc]
+        return remote(slot, slot, ds_sem, dr_sem.at[k], at_c)
 
     def r1_copy(k, v, h):
         start, size = out_cuts[h]
         cols = pl.ds(start, size)
         return remote(
-            part.at[k, 1 - c, v, :, cols], r1.at[k, v, :, cols], r1s_sem.at[k, v, h], r1r_sem.at[k, v, h], at_c
+            part.at[k, 1 - c, v, :, cols], r1.at[k, v, :, cols], r1s_sem, r1r_sem.at[k, v, h], at_c
         )
 
-    def r2_copy(k, q):
-        return remote(r2s.at[k, chunk(q)], r2r.at[k, chunk(q)], r2s_sem.at[k, q], r2r_sem.at[k, q], at_y)
-
-    def r3_copy(k, q):
-        return remote(r3s.at[k, chunk(q)], home.at[z, chunk(q)], r3s_sem.at[k, q], r3r_sem.at[z, q], at_z(k))
-
-    def r3_arrival(k, q):
+    def piece(u):
+        cols = pl.ds(pl.multiple_of(u // nq * (width // 2), width // 2), width // 2)
+        return chunk(u % nq), cols
+
+    def r2_copy(k, u):
+        at = (k,) + piece(u)
+        return remote(r2s.at[at], r2r.at[at], r2s_sem, r2r_sem.at[k, u], at_y)
+
+    def r3_copy(k, u):
+        at = piece(u)
+        return remote(r3s.at[(k,) + at], home.at[(z,) + at], r3s_sem, r3r_sem.at[z], at_z(k))
+
+    def r3_arrival(k):
         p = peer(k)
-        return remote(r3s.at[k, chunk(q)], home.at[p, chunk(q)], r3s_sem.at[k, q], r3r_sem.at[p, q], at_z(k))
+        return remote(r3s.at[k], home.at[p], r3s_sem, r3r_sem.at[p], at_z(k))
 
     def forward_z(k, q):
         if k > 0:
@@ -254,41 +271,37 @@
         y_arrival(k, q).wait_recv()
         d_copy(k, q).start()
 
-    def chip_sum(k, q):
-        at = chunk(q)
-
-        @pl.when(q == 0)
-        def _():
-            for h in range(2):
-                r1_copy(k, 1 - y, h).wait_recv()
-
-        r2s[k, at, :] = (part[k, c, 1 - y, at, :].astype(f32) + r1[k, 1 - y, at, :].astype(f32)).astype(bf16)
-        r2_copy(k, q).start()
-
-    def group_sum(k, q):
-        at = chunk(q)
-
-        @pl.when(q == 0)
-        def _():
-            for h in range(2):
-                r1_copy(k, y, h).wait_recv()
-
-        r2_copy(k, q).wait_recv()
+    def r1_wait(k, v, u):
+        for h in range(2):
+            @pl.when(u == h * nq)
+            def _():
+                r1_copy(k, v, h).wait_recv()
+
+    def chip_sum(k, u):
+        at, cols = piece(u)
+        r1_wait(k, 1 - y, u)
+        r2s[k, at, cols] = (
+            part[k, c, 1 - y, at, cols].astype(f32) + r1[k, 1 - y, at, cols].astype(f32)
+        ).astype(bf16)
+        r2_copy(k, u).start()
+
+    def group_sum(k, u):
+        at, cols = piece(u)
+        r1_wait(k, y, u)
+        r2_copy(k, u).wait_recv()
         total = (
-            part[k, c, y, at, :].astype(f32) + r1[k, y, at, :].astype(f32) + r2r[k, at, :].astype(f32)
+            part[k, c, y, at, cols].astype(f32) + r1[k, y, at, cols].astype(f32) + r2r[k, at, cols].astype(f32)
         ).astype(bf16)
         if k == 0:
-            home[z, at, :] = total
+            home[z, at, cols] = total
         else:
-            r3s[k, at, :] = total
-            r3_copy(k, q).start()
+            r3s[k, at, cols] = total
+            r3_copy(k, u).start()
 
     def mix(k):
         e = peer(k)
         if k > 0:
-            @pl.loop(0, nq)
-            def _(q):
-                r3_arrival(k, q).wait_recv()
+            r3_arrival(k).wait_recv()
 
         slot = jnp.sum(jnp.where(lane == e, rank, 0.0), axis=1, keepdims=True)
         share = jnp.sum(jnp.where(lane == e, weight_c, 0.0), axis=1, keepdims=True)
@@ -339,34 +352,40 @@
     def _(k):
         dispatch(peer(k), disp.at[k])
 
-        @pl.when((k == 1) | (inner & (k == 2)))
+        @pl.when((k == 1) | (inner & (k == experts - 1)))
         def _():
             send_z(k)
 
     acc[...] = jnp.zeros_like(acc)
 
-    @pl.loop(0, nq)
+    lead = min(2, nq)
+
+    @pl.loop(0, lead)
     def _(q):
         forward_y(0, q)
-        if experts > 1:
-            forward_z(1, q)
+
+    @pl.loop(lead, nq)
+    def _(q):
+        forward_z(1, q - lead)
+        forward_y(0, q)
+
+    @pl.loop(nq - lead, nq)
+    def _(q):
+        forward_z(1, q)
 
     @pl.loop(2, experts)
     def _(k):
-        @pl.when(edge | (k > 2))
+        @pl.when(edge | (k < experts - 1))
         def _():
             send_z(k)
 
-    for which in range(3):
-        for copy in weight(which):
-            copy.wait()
+    for which, (hbm, vmem) in enumerate(((wg_hbm, wg), (wu_hbm, wu), (wd_hbm, wd))):
+        pltpu.make_async_copy(hbm, vmem, w_sem.at[which]).wait()
 
     @pl.loop(0, experts)
     def _(k):
-        @pl.loop(0, nq)
-        def _(q):
-            c_arrival(k, q).wait_recv()
-            d_arrival(k, q).wait_recv()
+        c_arrival(k).wait_recv()
+        d_arrival(k).wait_recv()
 
         for h, (start, size) in enumerate(ff_cuts):
             cols = slice(start, start + size)
@@ -395,25 +414,14 @@
 
     out_ref[...] = acc[...].astype(bf16)
 
-    @pl.loop(0, experts)
-    def _(k):
-        @pl.when(k > 0)
-        def _():
-            @pl.loop(0, nq)
-            def _(q):
-                z_copy(k, q).wait_send()
-                r3_copy(k, q).wait_send()
-
-        @pl.loop(0, nq)
-        def _(q):
-            y_copy(k, q).wait_send()
-            c_copy(k, q).wait_send()
-            d_copy(k, q).wait_send()
-            r2_copy(k, q).wait_send()
-
-        for v in range(2):
-            for h in range(2):
-                r1_copy(k, v, h).wait_send()
+    others = pl.ds(1, experts - 1)
+    remote(disp.at[others], disp.at[others], zs_sem, cr_sem.at[0], at_c).wait_send()
+    remote(disp, disp, ys_sem, cr_sem.at[0], at_c).wait_send()
+    remote(disp, disp, cs_sem, cr_sem.at[0], at_c).wait_send()
+    remote(disp, disp, ds_sem, cr_sem.at[0], at_c).wait_send()
+    remote(part.at[:, 0], r1, r1s_sem, cr_sem.at[0], at_c).wait_send()
+    remote(r2s, r2r, r2s_sem, cr_sem.at[0], at_c).wait_send()
+    remote(r3s.at[others], home.at[others], r3s_sem, cr_sem.at[0], at_c).wait_send()
 
 
 def local(tokens, norm_gain, expert_ids, mix_weights, gate_weight, up_weight, down_weight):
@@ -431,7 +439,7 @@
     block = (cap, width)
     return pl.pallas_call(
         functools.partial(kernel, experts),
-        out_shape=jax.ShapeDtypeStruct((rows, width), bf16),
+        out_shape=pltpu.VMEM((rows, width), bf16),
         in_specs=[vmem, vmem, vmem, vmem, hbm, hbm, hbm],
         out_specs=vmem,
         scratch_shapes=[
@@ -449,10 +457,12 @@
             pltpu.VMEM((experts,) + block, bf16),
             pltpu.VMEM((experts,) + block, bf16),
             pltpu.VMEM((rows, width), f32),
-            dma((3, 4)),
-        ] + [dma((experts, nq))] * 8 + [dma((experts, 2, 2))] * 2 + [dma((experts, nq))] * 4,
+            dma((3,)),
+                    dma, dma((experts, nq)), dma, dma((experts, nq)), dma, dma((experts,)), dma, dma((experts,)),
+            dma, dma((experts, 2, 2)), dma, dma((experts, 2 * nq)), dma, dma((experts,)),
+        ],
         compiler_params=pltpu.CompilerParams(
-            collective_id=0, has_side_effects=True, vmem_limit_bytes=64 * 1024 * 1024 - 65536,
+            collective_id=0, has_side_effects=True, vmem_limit_bytes=58 * 1024 * 1024,
         ),
     )(tokens, norm_gain.reshape(1, width), expert_ids.T, mix_weights.T, gate_weight, up_weight, down_weight)
 

time: 81.9 us -> 75.9 us (0.927)
  Pallas kernels: 79.9 us -> 74.9 us
  local copies, waits for them, and re-layouts: 1.88 us -> 0.8 us
    pallas_call x1, Pallas kernels: 79.9 us -> 74.9 us  [local(): pl.pallas_call(functools.partial(kernel, experts), out_shape=pltpu.VMEM((...]
    unnamed x1, local copies, waits for them, and re-layouts: 1.88 us -> 0.8 us
where the time goes in v3:
time: 75.9 us; the launch traced here: 75.7 us
  Pallas kernels  74.9 us (99%)
  local copies, waits for them, and re-layouts  0.8 us (1%)
    pallas_call x1, Pallas kernels, local(): pl.pallas_call(functools.partial(kernel, experts), out_shape=pltpu.VMEM((...  74.9 us

profile of v3, /device:TPU:0, one launch (start us, length us, event | category | flops | bytes accessed | tf_op | source)
XLA Modules:
  0.0 75.7 jit_solution(6434224332527539010)
XLA Ops:
  0.0 74.9 %shard_map.73 = bf16[128,2048]{1,0:T(8,128)(2,1)S(1)} custom-call(bf16[128,2048]{1,0:T(8,128)(2,1)} %tok_ref.1, f32[1,2048]{1,0:T(1,128)} %bitcast.3, s32[2,128]{1,0:T(2,128)} %bitcast.4, f32[2,128]{1,0:T(2,128)} %bitcast.5, bf16[2048,1792]{1,0:T(8,128)(2,1)} %wg_hbm.1, bf16[2048,1792]{1,0:T(8,128)(2,1)} %wu_hbm.1, bf16[1792,2048]{1,0:T(8,128)(2,1)} %wd_hbm.1), custom_call_target="tpu_custom_call" | custom-call | tf_op jit(solution)/shard_map/pallas_call | solution.py:440
  74.9 0.8 %copy.9 = bf16[128,2048]{1,0:T(8,128)(2,1)} copy(bf16[128,2048]{1,0:T(8,128)(2,1)S(1)} %shard_map.73) | data formatting | bytes 1048576

commit v4 on v3

--- a/solution.py
+++ b/solution.py
@@ -33,7 +33,8 @@
 
         def at(step, place, *items, ev=ev):
             ev.setdefault((step, place), []).extend(
-                (kind, k, nq * lo // 5, nq * hi // 5) for kind, k, lo, hi in items
+                item if item[0] == "end" else (item[0], item[1], nq * item[2] // 5, nq * item[3] // 5)
+                for item in items
             )
 
         if experts == 4:
@@ -54,46 +55,46 @@
                 at(2, 5, ("chip", 2, 0, 5), ("group", 1, 8, 10), ("chip", 2, 5, 10))
                 at(3, 1, ("group", 2, 0, 1))
                 at(3, 2, ("group", 2, 1, 4))
-                at(3, 3, ("group", 2, 4, 7))
-                at(3, 4, ("chip", 0, 3, 5), ("group", 2, 7, 9))
+                at(3, 3, ("chip", 0, 3, 6), ("group", 2, 4, 7))
+                at(3, 4, ("group", 2, 7, 9))
                 at(3, 5, ("chip", 3, 0, 5), ("group", 2, 9, 10))
-                at(4, 0, ("chip", 3, 5, 10), ("chip", 0, 5, 10), ("group", 0, 0, 5))
-                at(4, 0, ("mix", 1, 0, 5), ("group", 3, 0, 10), ("group", 0, 5, 10))
-                at(4, 0, ("mix", 0, 0, 5), ("mix", 3, 0, 5), ("mix", 2, 0, 5))
+                at(4, 0, ("chip", 3, 5, 10), ("group", 0, 0, 6))
+                at(4, 0, ("mix", 1, 0, 5), ("group", 3, 0, 6), ("chip", 0, 6, 10), ("group", 3, 6, 10))
+                at(4, 0, ("group", 0, 6, 10), ("mix", 0, 0, 5), ("end", 3, 2))
             else:
-                at(0, 2, ("z", 2, 0, 1))
-                at(0, 3, ("z", 2, 1, 2), ("y", 1, 0, 4))
-                at(0, 4, ("y", 1, 4, 5), ("z", 2, 2, 4))
-                at(0, 5, ("z", 2, 4, 5))
-                at(1, 1, ("chip", 0, 0, 4))
-                at(1, 3, ("chip", 0, 4, 6), ("y", 2, 0, 5))
-                at(1, 4, ("z", 3, 0, 1))
-                at(1, 5, ("z", 3, 1, 2))
-                at(2, 1, ("z", 3, 2, 4))
-                at(2, 2, ("z", 3, 4, 5))
-                at(2, 3, ("chip", 1, 0, 2), ("y", 3, 0, 2))
-                at(2, 4, ("chip", 1, 2, 4), ("y", 3, 2, 5))
-                at(2, 5, ("chip", 2, 0, 10))
-                at(3, 1, ("group", 1, 0, 4))
-                at(3, 2, ("group", 2, 0, 2))
-                at(3, 3, ("group", 2, 2, 5))
-                at(3, 4, ("chip", 1, 4, 7), ("group", 2, 5, 8))
-                at(3, 5, ("chip", 3, 0, 5), ("group", 2, 8, 9))
-                at(4, 0, ("chip", 3, 5, 10), ("chip", 1, 7, 10), ("chip", 0, 6, 10), ("group", 2, 9, 10))
-                at(4, 0, ("group", 1, 4, 7), ("group", 0, 0, 6), ("group", 3, 0, 10), ("mix", 2, 0, 5))
-                at(4, 0, ("group", 1, 7, 10), ("group", 0, 6, 10))
-                at(4, 0, ("mix", 0, 0, 5), ("mix", 3, 0, 5), ("mix", 1, 0, 5))
+                at(0, 2, ("z", 1, 0, 1))
+                at(0, 3, ("z", 1, 1, 2), ("y", 2, 0, 4))
+                at(0, 4, ("y", 2, 4, 5), ("z", 1, 2, 4))
+                at(0, 5, ("z", 1, 4, 5), ("y", 1, 0, 3), ("chip", 0, 0, 4), ("y", 1, 3, 5))
+                at(1, 1, ("chip", 0, 4, 6))
+                at(1, 2, ("z", 3, 0, 1))
+                at(1, 3, ("z", 3, 1, 2))
+                at(1, 4, ("z", 3, 2, 4))
+                at(1, 5, ("z", 3, 4, 5), ("chip", 1, 0, 10))
+                at(2, 2, ("y", 3, 0, 5))
+                at(2, 3, ("group", 1, 0, 3))
+                at(2, 4, ("group", 1, 3, 5))
+                at(2, 5, ("chip", 2, 0, 5), ("group", 1, 5, 7))
+                at(3, 1, ("chip", 2, 5, 10), ("group", 1, 7, 9))
+                at(3, 2, ("group", 1, 9, 10))
+                at(3, 3, ("group", 2, 0, 3))
+                at(3, 4, ("chip", 0, 6, 9), ("group", 2, 3, 5))
+                at(3, 5, ("chip", 3, 0, 5), ("group", 2, 5, 7))
+                at(4, 0, ("chip", 3, 5, 10), ("chip", 0, 9, 10), ("group", 2, 7, 10), ("group", 0, 0, 9))
+                at(4, 0, ("group", 3, 0, 10), ("group", 0, 9, 10))
+                at(4, 0, ("mix", 1, 0, 5), ("mix", 0, 0, 5), ("end", 3, 2))
         else:
             for k in range(experts):
                 if k + 2 < experts:
-                    at(k, 2, ("z", k + 2, 0, 5))
+                    at(k, 2, ("z", k + 2 if inner or k else 1, 0, 5))
                 if k + 1 < experts:
                     at(k, 5, ("y", k + 1, 0, 5))
                 if k > 0:
                     at(k, 1, ("chip", k - 1, 0, 10))
                     at(k, 3, ("group", k - 1, 0, 10))
             at(experts, 0, ("chip", last, 0, 10), ("group", last, 0, 10))
-            at(experts, 0, *[("mix", k, 0, 5) for k in range(experts)])
+            at(experts, 0, *[("mix", k, 0, 5) for k in range(experts - 2)])
+            at(experts, 0, ("end", experts - 2, last))
         tail = ev.pop((experts, 0))
         sides.append((ev, tail))
     return sides
@@ -101,8 +102,9 @@
 
 def kernel(
     experts,
-    tok_ref, gain_ref, ids_ref, mix_ref, wg_hbm, wu_hbm, wd_hbm,
+    tok_hbm, gain_hbm, ids_hbm, mix_hbm, wg_hbm, wu_hbm, wd_hbm,
     out_ref,
+    tok_ref, gain_ref, ids_ref, mix_ref, in_sem,
     wg, wu, wd, normed, disp, xin, hid, part, r1, r2s, r2r, r3s, home, acc,
     w_sem, zs_sem, zr_sem, ys_sem, yr_sem, cs_sem, cr_sem, ds_sem, dr_sem,
     r1s_sem, r1r_sem, r2s_sem, r2r_sem, r3s_sem, r3r_sem,
@@ -127,8 +129,12 @@
     inner = near > 0
     edge = near == 0
 
+    beside = min(2, experts - 1)
+
     def peer(k):
-        from_edge = z + away * jnp.where(k < 2, k, experts + 1 - k)
+        from_edge = z + away * jnp.where(
+            k == 0, 0, jnp.where(k == beside, 1, jnp.where(k == 1, experts - 1, experts + 1 - k))
+        )
         n = jnp.where(k < 2, k, jnp.where(k == experts - 1, 2, k + 1))
         both = z + away * ((n + 1) // 2) * (2 * (n % 2) - 1)
         from_inner = jnp.where(n <= 2 * near, both, z + away * (n - near))
@@ -165,6 +171,18 @@
         pl.semaphore_signal(barrier, inc=1, device_id=at_z(k), device_id_type=pl.DeviceIdType.MESH)
     pl.semaphore_signal(barrier, inc=1, device_id=at_y, device_id_type=pl.DeviceIdType.MESH)
     pl.semaphore_signal(barrier, inc=1, device_id=at_c, device_id_type=pl.DeviceIdType.MESH)
+
+    inputs_in = [
+        pltpu.make_async_copy(src, dst, in_sem.at[i])
+        for i, (src, dst) in enumerate(
+            ((ids_hbm, ids_ref), (mix_hbm, mix_ref), (gain_hbm, gain_ref), (tok_hbm, tok_ref))
+        )
+    ]
+    for copy in inputs_in:
+        copy.start()
+
+    for copy in inputs_in:
+        copy.wait()
 
     for which in range(3):
         for copy in weight(which):
@@ -298,19 +316,30 @@
             r3s[k, at, cols] = total
             r3_copy(k, u).start()
 
-    def mix(k):
+    def shares(k):
         e = peer(k)
-        if k > 0:
-            r3_arrival(k).wait_recv()
-
         slot = jnp.sum(jnp.where(lane == e, rank, 0.0), axis=1, keepdims=True)
         share = jnp.sum(jnp.where(lane == e, weight_c, 0.0), axis=1, keepdims=True)
         place = lax.broadcasted_iota(jnp.int32, (rows, cap), 1)
         pick = (place == slot.astype(jnp.int32)).astype(f32).astype(bf16)
+        return e, share, pick
+
+    def mix(*blocks, last=False):
+        for k in blocks:
+            if k > 0:
+                r3_arrival(k).wait_recv()
+
+        parts = [shares(k) for k in blocks]
         wide = tile_of(width, 512)
         for n in range(width // wide):
             cols = slice(n * wide, (n + 1) * wide)
-            acc[:, cols] += share * jnp.dot(pick, home[e, :, cols], preferred_element_type=f32)
+            total = acc[:, cols]
+            for e, share, pick in parts:
+                total += share * jnp.dot(pick, home[e, :, cols], preferred_element_type=f32)
+            if last:
+                out_ref[:, cols] = total.astype(bf16)
+            else:
+                acc[:, cols] = total
 
     actions = {"z": forward_z, "y": forward_y, "chip": chip_sum, "group": group_sum}
     sides = plan(experts, nq)
@@ -319,6 +348,8 @@
         for item in items:
             if item[0] == "mix":
                 mix(item[1])
+            elif item[0] == "end":
+                mix(item[1], item[2], last=True)
             else:
                 kind, k, lo, hi = item
 
@@ -352,11 +383,20 @@
     def _(k):
         dispatch(peer(k), disp.at[k])
 
-        @pl.when((k == 1) | (inner & (k == experts - 1)))
+        @pl.when(jnp.where(inner, (k == 1) | (k == experts - 1), k == beside))
         def _():
             send_z(k)
 
     acc[...] = jnp.zeros_like(acc)
+
+    def forward_near(q):
+        @pl.when(inner)
+        def _():
+            forward_z(1, q)
+
+        @pl.when(edge)
+        def _():
+            forward_z(beside, q)
 
     lead = min(2, nq)
 
@@ -366,16 +406,16 @@
 
     @pl.loop(lead, nq)
     def _(q):
-        forward_z(1, q - lead)
+        forward_near(q - lead)
         forward_y(0, q)
 
     @pl.loop(nq - lead, nq)
     def _(q):
-        forward_z(1, q)
-
-    @pl.loop(2, experts)
+        forward_near(q)
+
+    @pl.loop(1, experts)
     def _(k):
-        @pl.when(edge | (k < experts - 1))
+        @pl.when(jnp.where(inner, (k > 1) & (k < experts - 1), k != beside))
         def _():
             send_z(k)
 
@@ -412,7 +452,6 @@
             def _():
                 perform(items)
 
-    out_ref[...] = acc[...].astype(bf16)
 
     others = pl.ds(1, experts - 1)
     remote(disp.at[others], disp.at[others], zs_sem, cr_sem.at[0], at_c).wait_send()
@@ -440,9 +479,14 @@
     return pl.pallas_call(
         functools.partial(kernel, experts),
         out_shape=pltpu.VMEM((rows, width), bf16),
-        in_specs=[vmem, vmem, vmem, vmem, hbm, hbm, hbm],
+        in_specs=[hbm] * 7,
         out_specs=vmem,
         scratch_shapes=[
+            pltpu.VMEM((rows, width), bf16),
+            pltpu.VMEM((1, width), f32),
+            pltpu.VMEM((top, rows), jnp.int32),
+            pltpu.VMEM((top, rows), f32),
+            dma((4,)),
             pltpu.VMEM((width, ff), bf16),
             pltpu.VMEM((width, ff), bf16),
             pltpu.VMEM((ff, width), bf16),

time: 75.9 us -> 73.3 us (0.966)
  Pallas kernels: 74.9 us -> 72.3 us
    pallas_call x1, Pallas kernels: 74.9 us -> 72.3 us  [local(): pl.pallas_call(functools.partial(kernel, experts), out_shape=pltpu.VMEM((...]
where the time goes in v4:
time: 73.3 us; the launch traced here: 73.1 us
  Pallas kernels  72.3 us (99%)
  local copies, waits for them, and re-layouts  0.8 us (1%)
    pallas_call x1, Pallas kernels, local(): pl.pallas_call(functools.partial(kernel, experts), out_shape=pltpu.VMEM((...  72.3 us

profile of v4, /device:TPU:0, one launch (start us, length us, event | category | flops | bytes accessed | tf_op | source)
XLA Modules:
  0.0 73.1 jit_solution(9233058524237441192)
XLA Ops:
  0.0 72.3 %shard_map.73 = bf16[128,2048]{1,0:T(8,128)(2,1)S(1)} custom-call(bf16[128,2048]{1,0:T(8,128)(2,1)} %tok_hbm.1, f32[1,2048]{1,0:T(1,128)} %bitcast.3, s32[2,128]{1,0:T(2,128)} %bitcast.4, f32[2,128]{1,0:T(2,128)} %bitcast.5, bf16[2048,1792]{1,0:T(8,128)(2,1)} %wg_hbm.1, bf16[2048,1792]{1,0:T(8,128)(2,1)} %wu_hbm.1, bf16[1792,2048]{1,0:T(8,128)(2,1)} %wd_hbm.1), custom_call_target="tpu_custom_call" | custom-call | tf_op jit(solution)/shard_map/pallas_call | solution.py:479
  72.3 0.8 %copy.9 = bf16[128,2048]{1,0:T(8,128)(2,1)} copy(bf16[128,2048]{1,0:T(8,128)(2,1)S(1)} %shard_map.73) | data formatting | bytes 1048576
